TPU v7x, 32 devices: a whole 2x2x4 slice. The times are simulated.
32 devices in a mesh: sp: 4 (over z), fs: 4 (over y, x), tp: 2 (over core).
Axes of the slice: x: 2, y: 2, z: 4, core: 2. Of those that a mesh axis runs over, the one named last changes fastest.
Arguments:
- state_head_inputs: bfloat16 [4, 512, 1024], P('fs', 'sp', 'tp'), may hold values from -6 to 6
- state_write_vectors: bfloat16 [4, 512, 256], P('fs', 'sp', 'tp'), may hold values from -3 to 3
- state_read_vectors: bfloat16 [4, 512, 256], P('fs', 'sp', 'tp'), may hold values from -3 to 3
- state_output_gate: bfloat16 [4, 512, 1024], P('fs', 'sp', 'tp'), may hold values from -6 to 6
- presoftplus_steps: float32 [4, 16, 512], P('fs', 'tp', 'sp'), may hold values from -6 to 6
- extra_decay_log: float32 [4, 16, 512], P('fs', 'tp', 'sp'), may hold values from -2.1 to 0, as said below
- lane_shrinkage_powers: float32 [16], P('tp')
- bypass_coefficient_vector: float32 [16], P('tp'), may hold values from 0.5 to 4
- feeder_smoothing_stencil: bfloat16 [4, 1024], P(None, 'tp'), may hold values from -3 to 3
- stored_smoothing_stencil: bfloat16 [4, 256], P(None, 'tp'), may hold values from -3 to 3
- lookup_smoothing_stencil: bfloat16 [4, 256], P(None, 'tp'), may hold values from -3 to 3
- bundled_rescaling_vector: float32 [1024], P('tp'), may hold values from 0.1 to 1.9
- queries: bfloat16 [4, 512, 1024], P('fs', 'sp', 'tp'), may hold values from -8 to 8
- attention_keys: bfloat16 [4, 512, 256], P('fs', 'sp', 'tp'), may hold values from -8 to 8
- attention_values: bfloat16 [4, 512, 256], P('fs', 'sp', 'tp'), may hold values from -6 to 6
- forget_gate_cumsum: float32 [4, 512, 16], P('fs', 'sp', 'tp'), as said below
- state_out_weight: bfloat16 [1024, 2048], P('tp', 'fs'), may hold values from -0.1875 to 0.1875
- attention_out_weight: bfloat16 [1024, 2048], P('tp', 'fs'), may hold values from -0.75 to 0.75
Outputs:
- layer_output: bfloat16 [4, 512, 2048], P('fs', ('sp', 'tp'))
Inputs may be any that keep to these rules, and one draw needn't show every extreme that they name: `extra_decay_log`: nonpositive. `forget_gate_cumsum`: never rises along the positions of a sequence.
All inputs are finite; a program needn't handle non-finite values.
Results may differ from a plain program's by a relative error of at most 0.019.
Values may be sent and summed in bfloat16 or wider, within the bound.
A program may use at most 64 MiB of HBM per device.

v0:
```python
import math
import jax
import jax.numpy as jnp
from jax import lax
from jax.sharding import PartitionSpec as P

HEAD_DIM = 64
STATE = 128
EPSILON = 1e-06
NEGATIVE = -1e30


def passed_along(shard, axis, by):
    devices = lax.axis_size(axis)
    pairs = [(i, i + by) for i in range(devices) if 0 <= i + by < devices]
    return lax.ppermute(shard, axis, pairs)


def entering(shard, axis, join, neutral):
    place = lax.axis_index(axis)
    gathered = jax.tree.map(
        lambda a, kind: lax.all_gather(a.astype(kind), axis), shard, (jnp.bfloat16, jnp.bfloat16)
    )
    state = jax.tree.map(lambda a, e: jnp.zeros_like(a) + jnp.asarray(e, a.dtype), shard, neutral)

    def one(hop, state):
        return join(
            state,
            jax.tree.map(
                lambda a, own: lax.dynamic_index_in_dim(a, hop, 0, False).astype(own.dtype),
                gathered,
                shard,
            ),
        )

    return lax.fori_loop(0, place, one, state)


def causal_filter(feeder_quantities, before, taps):
    length = feeder_quantities.shape[0]
    padded = jnp.concatenate([before, feeder_quantities], axis=0).astype(jnp.float32)
    summed = jnp.zeros(feeder_quantities.shape, jnp.float32)
    for offset in range(taps.shape[0]):
        summed = summed + taps[offset].astype(jnp.float32) * padded[offset : offset + length]
    return jax.nn.silu(summed).astype(jnp.bfloat16)


def compose(earlier, later):
    return (earlier[0] * later[0], earlier[1] * later[0][..., None, None] + later[1])


def shards(
    state_head_inputs,
    state_write_vectors,
    state_read_vectors,
    state_output_gate,
    presoftplus_steps,
    extra_decay_log,
    lane_shrinkage_powers,
    bypass_coefficient_vector,
    feeder_smoothing_stencil,
    stored_smoothing_stencil,
    lookup_smoothing_stencil,
    bundled_rescaling_vector,
    queries,
    attention_keys,
    attention_values,
    forget_gate_cumsum,
    state_out_weight,
    attention_out_weight,
):
    shard_rows = state_head_inputs.shape[1]
    input_rows = state_head_inputs[0]
    write_rows = state_write_vectors[0]
    read_rows = state_read_vectors[0]
    tap_rows = feeder_smoothing_stencil.shape[0] - 1
    value_width = input_rows.shape[1]
    vector_width = write_rows.shape[1]
    tail_rows = jnp.concatenate(
        [input_rows[-tap_rows:], write_rows[-tap_rows:], read_rows[-tap_rows:]], axis=1
    )
    before = passed_along(tail_rows, "sp", 1)
    conv_values = causal_filter(input_rows, before[:, :value_width], feeder_smoothing_stencil)
    conv_write = causal_filter(
        write_rows, before[:, value_width : value_width + vector_width], stored_smoothing_stencil
    )
    conv_read = causal_filter(
        read_rows, before[:, value_width + vector_width :], lookup_smoothing_stencil
    )
    stride_duration = jax.nn.softplus(presoftplus_steps[0])
    shrinkage_natural_power = (
        stride_duration * (-jnp.exp(lane_shrinkage_powers))[:, None] + extra_decay_log[0]
    )
    lane_tally = stride_duration.shape[0]
    groups = vector_width // STATE
    per_group = lane_tally // groups
    cumulative = jnp.cumsum(shrinkage_natural_power, axis=1)
    input_heads = conv_values.reshape(shard_rows, groups, per_group, HEAD_DIM)
    write_groups = conv_write.reshape(shard_rows, groups, STATE)
    read_groups = conv_read.reshape(shard_rows, groups, STATE)
    inner_products = jnp.einsum(
        "tgn,sgn->gts", read_groups, write_groups, preferred_element_type=jnp.float32
    )
    positions = jnp.arange(shard_rows)
    causal = positions[:, None] >= positions[None, :]
    log_gap = jnp.where(causal[None], cumulative[:, :, None] - cumulative[:, None, :], -jnp.inf)
    weights = jnp.exp(log_gap) * stride_duration[:, None, :]
    mix_weights = (
        inner_products[:, None] * weights.reshape(groups, per_group, shard_rows, shard_rows)
    ).astype(jnp.bfloat16)
    local_part = jnp.einsum(
        "ghts,sghp->tghp", mix_weights, input_heads, preferred_element_type=jnp.float32
    )
    end_scale = (jnp.exp(cumulative[:, -1:] - cumulative) * stride_duration).T.reshape(
        shard_rows, groups, per_group
    )
    weighted = (input_heads.astype(jnp.float32) * end_scale[..., None]).astype(jnp.bfloat16)
    block_state = jnp.einsum(
        "sghp,sgn->ghpn", weighted, write_groups, preferred_element_type=jnp.float32
    )
    total_decay = jnp.exp(cumulative[:, -1]).reshape(groups, per_group)
    identity = (jnp.ones_like(total_decay), jnp.zeros_like(block_state))
    carried = entering((total_decay, block_state), "sp", compose, identity)[1]
    carried_part = jnp.einsum(
        "tgn,ghpn->tghp",
        read_groups,
        carried.astype(jnp.bfloat16),
        preferred_element_type=jnp.float32,
    )
    carried_part = (
        carried_part * jnp.exp(cumulative).T.reshape(shard_rows, groups, per_group)[..., None]
    )
    mixer_sum = (
        local_part
        + carried_part
        + bypass_coefficient_vector.reshape(groups, per_group)[None, :, :, None]
        * input_heads.astype(jnp.float32)
    )
    gated_rows = mixer_sum.reshape(shard_rows, groups, per_group * HEAD_DIM) * jax.nn.silu(
        state_output_gate[0].astype(jnp.float32)
    ).reshape(shard_rows, groups, -1)
    stretch_coefficient = lax.rsqrt(
        jnp.mean(gated_rows * gated_rows, axis=-1, keepdims=True) + EPSILON
    )
    state_result = (
        (gated_rows * stretch_coefficient * bundled_rescaling_vector.reshape(groups, -1))
        .reshape(shard_rows, -1)
        .astype(jnp.bfloat16)
    )
    attend_heads = forget_gate_cumsum.shape[2]
    key_group_count = attention_keys.shape[2] // HEAD_DIM
    repeat_factor = attend_heads // key_group_count
    query_head_count = queries[0].reshape(shard_rows, key_group_count, repeat_factor, HEAD_DIM)
    first_query = lax.axis_index("sp") * shard_rows
    query_index = first_query + jnp.arange(shard_rows)
    last_query = first_query + shard_rows - 1
    query_gates = forget_gate_cumsum[0].T
    all_gates = lax.all_gather(forget_gate_cumsum[0], "sp", axis=0, tiled=True)
    attention_score_scale = HEAD_DIM ** (-0.5)
    starting = (
        jnp.full((attend_heads, shard_rows), NEGATIVE, jnp.float32),
        jnp.zeros((attend_heads, shard_rows), jnp.float32),
        jnp.zeros((attend_heads, shard_rows, HEAD_DIM), jnp.float32),
    )
    key_rows = lax.all_gather(attention_keys[0], "sp", axis=0, tiled=True)
    value_rows = lax.all_gather(attention_values[0], "sp", axis=0, tiled=True)
    span = key_rows.shape[0]
    sub_block = math.gcd(span, 512)

    def advance(sub_index, running):
        first_key = sub_index * sub_block

        def attend(running):
            running_max, running_sum, weighted_sum = running
            key_tile = lax.dynamic_slice_in_dim(
                key_rows, sub_index * sub_block, sub_block, 0
            ).reshape(sub_block, key_group_count, HEAD_DIM)
            value_tile = lax.dynamic_slice_in_dim(
                value_rows, sub_index * sub_block, sub_block, 0
            ).reshape(sub_block, key_group_count, HEAD_DIM)
            key_gates = lax.dynamic_slice_in_dim(all_gates, first_key, sub_block, 0)
            attention_scores = jnp.einsum(
                "ezxp,czp->zxec", query_head_count, key_tile, preferred_element_type=jnp.float32
            )
            attention_scores = (
                attention_scores.reshape(attend_heads, shard_rows, sub_block)
                * attention_score_scale
            )
            attention_scores = attention_scores + query_gates[:, :, None] - key_gates.T[:, None, :]
            visible = (first_key + jnp.arange(sub_block))[None, :] <= query_index[:, None]
            attention_scores = jnp.where(visible[None], attention_scores, NEGATIVE)
            new_max = jnp.maximum(running_max, jnp.max(attention_scores, axis=-1))
            shrink = jnp.exp(running_max - new_max)
            attention_probs = jnp.where(
                visible[None], jnp.exp(attention_scores - new_max[..., None]), 0.0
            )
            running_sum = running_sum * shrink + jnp.sum(attention_probs, axis=-1)
            weighted_value_sum = jnp.einsum(
                "fljx,xfc->fljc",
                attention_probs.astype(jnp.bfloat16).reshape(
                    key_group_count, repeat_factor, shard_rows, sub_block
                ),
                value_tile,
                preferred_element_type=jnp.float32,
            )
            weighted_sum = weighted_sum * shrink[..., None] + weighted_value_sum.reshape(
                attend_heads, shard_rows, HEAD_DIM
            )
            return (new_max, running_sum, weighted_sum)

        return lax.cond(first_key <= last_query, attend, lambda kept: kept, running)

    _, running_sum, weighted_sum = lax.fori_loop(0, span // sub_block, advance, starting)
    attend_out = (
        (weighted_sum / running_sum[..., None])
        .transpose(1, 0, 2)
        .reshape(shard_rows, -1)
        .astype(jnp.bfloat16)
    )
    state_columns, attend_columns = (
        lax.all_gather(state_out_weight, "fs", axis=1, tiled=True),
        lax.all_gather(attention_out_weight, "fs", axis=1, tiled=True),
    )
    summed = lax.psum_scatter(
        (
            jnp.dot(state_result, state_columns, preferred_element_type=jnp.float32)
            + jnp.dot(attend_out, attend_columns, preferred_element_type=jnp.float32)
        ).astype(jnp.bfloat16),
        "tp",
        scatter_dimension=0,
        tiled=True,
    )
    return summed[None]


def solution(mesh):
    in_specs = (
        P("fs", "sp", "tp"),
        P("fs", "sp", "tp"),
        P("fs", "sp", "tp"),
        P("fs", "sp", "tp"),
        P("fs", "tp", "sp"),
        P("fs", "tp", "sp"),
        P("tp"),
        P("tp"),
        P(None, "tp"),
        P(None, "tp"),
        P(None, "tp"),
        P("tp"),
        P("fs", "sp", "tp"),
        P("fs", "sp", "tp"),
        P("fs", "sp", "tp"),
        P("fs", "sp", "tp"),
        P("tp", "fs"),
        P("tp", "fs"),
    )
    out_specs = P("fs", ("sp", "tp"), None)
    return jax.shard_map(shards, mesh=mesh, in_specs=in_specs, out_specs=out_specs, check_vma=False)
```

profile of v0, /device:TPU:0, one launch (start us, length us, event | category | flops | bytes accessed | tf_op | source)
XLA Modules:
  0.0 108.5 jit_solution(7209099858633542223)
XLA Ops:
  6.5 0.7 all-gather.8.cloned.1.call-update
  7.3 0.7 slice_bitcast_fusion.1
  8.0 0.7 slice_bitcast_fusion
  8.9 5.0 %collective-permute-start = (bf16[3,768]{0,1:T(8,128)(2,1)S(1)}, bf16[3,768]{0,1:T(8,128)(2,1)S(1)}, u32[]{:S(2)}, u32[]{:S(2)}) collective-permute-start(bf16[3,768]{0,1:T(8,128)(2,1)S(1)} %copy.46), channel_id=1, source_target_pairs={{0,8},{8,16},{16,24},{1,9},{9,17},{17,25},{2,10},{10,18},{18,26},{... | collective-permute-start | bytes 13832 | tf_op jit(solution)/shard_map/ppermute | solution.py:16
  14.0 0.7 exponential_negate_fusion
  14.6 0.8 compare_select_fusion
  15.4 0.3 reduce_window_sum.11
  15.7 0.2 slice_reduce_fusion
  15.9 0.8 multiply_bitcast_fusion
  16.7 0.8 slice_convert_fusion.3
  17.5 0.8 bitcast_convert_fusion.4
  18.3 0.8 bitcast_convert_fusion.8
  19.2 0.9 copy.53
  20.0 12.7 %all-gather.2 = bf16[1,512,128]{1,2,0:T(8,128)(2,1)S(1)} all-gather(bf16[1,128,128]{1,2,0:T(8,128)(2,1)S(1)} %copy.53), channel_id=4, replica_groups=mesh['sp'=4,'fs'=4,'tp'=2] {'sp'}, dimensions={1}, use_global_device_ids=true | all-gather | bytes 163840 | tf_op jit(solution)/shard_map/all_gather | solution.py:165
  32.8 13.3 %all-gather.3 = f32[1,512,8]{1,2,0:T(8,128)S(1)} all-gather(f32[1,128,8]{1,2,0:T(8,128)} %param.37), channel_id=5, replica_groups=mesh['sp'=4,'fs'=4,'tp'=2] {'sp'}, dimensions={1}, use_global_device_ids=true | all-gather | bytes 20480 | tf_op jit(solution)/shard_map/all_gather | solution.py:158
  46.1 0.9 copy.54
  47.0 12.3 %all-gather.4 = bf16[1,512,128]{1,2,0:T(8,128)(2,1)S(1)} all-gather(bf16[1,128,128]{1,2,0:T(8,128)(2,1)S(1)} %copy.54), channel_id=6, replica_groups=mesh['sp'=4,'fs'=4,'tp'=2] {'sp'}, dimensions={1}, use_global_device_ids=true | all-gather | bytes 163840 | tf_op jit(solution)/shard_map/all_gather | solution.py:166
  59.3 1.9 %conditional.1 = ((f32[8,128]{1,0:T(8,128)S(1)}, f32[8,128,64]{1,2,0:T(8,128)S(1)})) conditional(s32[]{:T(128)} %convert_element_type.195, (f32[8,128]{1,0:T(8,128)S(1)}, f32[8,128,64]{1,2,0:T(8,128)S(1)}) %tuple.33, (s32[]{:T(128)}, s32[128]{0:T(128)S(1)}, bf16[512,128]{0,1:T(8,128)(2,1)S(1)}, bf16[1,128,512]{2,1,0:T(8,128)(2,1)S(1)}, ...), branch_computations={%region_4.5_spmd, %region_5.8_spmd} | conditional | flops 140183680 | bytes 8361500 | solution.py:211
  59.6 0.8 fusion.47
  60.3 0.4 fusion.3
  60.7 0.5 fusion.4
  61.7 0.6 dynamic-slice
  62.9 0.2 dynamic-update-slice
  63.1 8.5 %all-reduce = bf16[32]{0:T(256)(128)(2,1)S(1)} all-reduce(bf16[32]{0:T(256)(128)(2,1)S(1)} %dynamic-update-slice), channel_id=2, replica_groups=mesh['sp'=4,'fs'=4,'tp'=2] {'sp'}, use_global_device_ids=true, to_apply=%add | all-reduce | flops 32 | bytes 128
  72.2 0.6 fusion.23
  72.9 14.8 %all-gather.1 = bf16[32,64,128]{2,1,0:T(8,128)(2,1)S(1)} all-gather(bf16[8,64,128]{2,1,0:T(8,128)(2,1)S(1)} %convolution_convert_fusion), channel_id=3, replica_groups=mesh['sp'=4,'fs'=4,'tp'=2] {'sp'}, dimensions={0}, use_global_device_ids=true | all-gather | bytes 655360 | tf_op jit(solution)/shard_map/all_gather | solution.py:22
  88.1 0.2 fusion.13
  88.3 0.4 copy-done.7
  88.7 0.4 multiply_reduce_fusion
  89.3 2.1 %fusion.50 = f32[128,2048]{1,0:T(8,128)S(1)} fusion(bf16[128,512]{0,1:T(8,128)(2,1)S(1)} %fusion.29, bf16[512,2048]{1,0:T(8,128)(2,1)} %all-gather.8.cloned.1.call-done), kind=kOutput, calls=%fused_computation.114 | convolution fusion | flops 268435456 | bytes 3276800 | tf_op jit(solution)/shard_map/dot_general | solution.py:226
  91.4 2.9 %fusion.10 = bf16[128,2048]{1,0:T(8,128)(2,1)} fusion(f32[128,2048]{1,0:T(8,128)S(1)} %fusion.50, bf16[128,512]{0,1:T(8,128)(2,1)S(1)} %bitcast.183, bf16[512,2048]{1,0:T(8,128)(2,1)} %all-gather.10.cloned.1.call-done), kind=kOutput, calls=%fused_computation.20 | convolution fusion | flops 268959744 | bytes 3801088 | tf_op jit(solution)/shard_map/dot_general | solution.py:227
  94.3 7.7 %reduce-scatter.2.cloned.1.call-done = bf16[64,2048]{1,0:T(8,128)(2,1)} async-done(((bf16[128,2048]{1,0:T(8,128)(2,1)}), bf16[64,2048]{1,0:T(8,128)(2,1)}) %reduce-scatter.2.cloned.1.call-update) | async-done | bytes 262160 | tf_op jit(solution)/shard_map/reduce_scatter | solution.py:224
  (59 shorter events, 2.2 us)
Async XLA Ops:
  6.5 52.8 %copy-start.5 = (f32[1,128,8]{1,2,0:T(8,128)S(1)}, f32[1,128,8]{1,2,0:T(8,128)}, u32[]{:S(2)}) copy-start(f32[1,128,8]{1,2,0:T(8,128)} %param.37) | copy-start | bytes 12292
  6.5 52.8 %copy-start.1 = (bf16[1,128,512]{2,1,0:T(8,128)(2,1)S(1)}, bf16[1,128,512]{2,1,0:T(8,128)(2,1)}, u32[]{:S(2)}) copy-start(bf16[1,128,512]{2,1,0:T(8,128)(2,1)} %param.34) | copy-start | bytes 393220
  6.5 82.7 %all-gather.8.cloned.1.call-start = ((), (), s32[]{:S(2)}) async-start(), calls=%async_computation.1 | async-start | bytes 2621440 | tf_op jit(solution)/shard_map/all_gather | solution.py:221
  7.3 84.1 %all-gather.10.cloned.1.call-start = ((), (), s32[]{:S(2)}) async-start(), calls=%async_computation.2 | async-start | bytes 2621440 | tf_op jit(solution)/shard_map/all_gather | solution.py:222
  8.9 62.9 %collective-permute-start = (bf16[3,768]{0,1:T(8,128)(2,1)S(1)}, bf16[3,768]{0,1:T(8,128)(2,1)S(1)}, u32[]{:S(2)}, u32[]{:S(2)}) collective-permute-start(bf16[3,768]{0,1:T(8,128)(2,1)S(1)} %copy.46), channel_id=1, source_target_pairs={{0,8},{8,16},{16,24},{1,9},{9,17},{17,25},{2,10},{10,18},{18,26},{... | collective-permute-start | bytes 13832 | tf_op jit(solution)/shard_map/ppermute | solution.py:16
  13.9 88.1 %reduce-scatter.2.cloned.1.call-start = ((), (), s32[]{:S(2)}) async-start(), calls=%async_computation.3 | async-start | bytes 786432 | tf_op jit(solution)/shard_map/reduce_scatter | solution.py:224
  59.3 2.2 %copy-start = (bf16[1,128,512]{2,1,0:T(8,128)(2,1)S(1)}, bf16[1,128,512]{2,1,0:T(8,128)(2,1)}, u32[]{:S(2)}) copy-start(bf16[1,128,512]{2,1,0:T(8,128)(2,1)} %param.22) | copy-start | bytes 393220
  59.3 2.4 %copy-start.8 = (u32[32]{0:T(128)S(1)}, u32[32]{0:T(128)}, u32[]{:S(2)}) copy-start(u32[32]{0:T(128)} %constant.96) | copy-start | bytes 388
  59.3 12.4 %copy-start.2 = (bf16[1,128,512]{2,1,0:T(8,128)(2,1)S(1)}, bf16[1,128,512]{2,1,0:T(8,128)(2,1)}, u32[]{:S(2)}) copy-start(bf16[1,128,512]{2,1,0:T(8,128)(2,1)} %param.25) | copy-start | bytes 393220
  61.3 10.8 %copy-start.3 = (bf16[1,128,128]{2,1,0:T(8,128)(2,1)S(1)}, bf16[1,128,128]{2,1,0:T(8,128)(2,1)}, u32[]{:S(2)}) copy-start(bf16[1,128,128]{2,1,0:T(8,128)(2,1)} %param.23) | copy-start | bytes 98308
  71.7 16.1 %copy-start.4 = (bf16[1,128,128]{2,1,0:T(8,128)(2,1)S(1)}, bf16[1,128,128]{2,1,0:T(8,128)(2,1)}, u32[]{:S(2)}) copy-start(bf16[1,128,128]{2,1,0:T(8,128)(2,1)} %param.24) | copy-start | bytes 98308
  88.0 0.7 copy-start.7
  88.1 1.0 copy-start.6
Sparse Core Ops, SparseCore 0:
  9.2 37.7 all-gather.7
  48.8 35.0 all-gather.9
  94.4 7.5 reduce-scatter.1
where the time goes:
time: 109 us
  blocking collectives  61.6 us (57%)
  between operations  14 us (13%)
  waiting for transfers between devices  8.53 us (8%)
  matrix products  7.06 us (6%)
  other arithmetic  6.77 us (6%)
  local copies, waits for them, and re-layouts  5.49 us (5%)
  starting transfers between devices  5.05 us (5%)
    all_gather x1, blocking collectives, entering(): lax.all_gather(a.astype(kind), axis)  14.8 us
    all_gather x1, blocking collectives, shards(): all_gates = lax.all_gather(forget_gate_cumsum[0], 'sp', axis=0, tiled=True)  13.3 us
    all_gather x1, blocking collectives, shards(): key_rows = lax.all_gather(attention_keys[0], 'sp', axis=0, tiled=True)  12.7 us
    all_gather x1, blocking collectives, shards(): value_rows = lax.all_gather(attention_values[0], 'sp', axis=0, tiled=True)  12.3 us
    unnamed x1, blocking collectives  8.49 us
    reduce_scatter x1, waiting for transfers between devices, shards(): lax.psum_scatter((jnp.dot(state_result, state_columns, preferred_element_...  7.74 us
    ppermute x1, starting transfers between devices, passed_along(): return lax.ppermute(shard, axis, pairs)  4.97 us
    unnamed x25, local copies, waits for them, and re-layouts  3.25 us
  transfers between devices with their start and end apart: 4, of which 1 were waited for; matrix products, arithmetic and copies ran while one was open for 15% of the time, Pallas kernels for 0%

commit v1 on v0

--- a/solution.py
+++ b/solution.py
@@ -155,7 +155,21 @@
     query_index = first_query + jnp.arange(shard_rows)
     last_query = first_query + shard_rows - 1
     query_gates = forget_gate_cumsum[0].T
-    all_gates = lax.all_gather(forget_gate_cumsum[0], "sp", axis=0, tiled=True)
+    ways, here, lap = (lax.axis_size("sp"), lax.axis_index("sp"), forget_gate_cumsum[0].shape[0])
+    shape = [n * ways if d == 0 else n for d, n in enumerate(forget_gate_cumsum[0].shape)]
+    full = lax.dynamic_update_slice_in_dim(
+        jnp.zeros(shape, forget_gate_cumsum[0].dtype), forget_gate_cumsum[0], here * lap, axis=0
+    )
+    going_up = going_down = forget_gate_cumsum[0]
+    for far in range(1, ways // 2 + 1):
+        going_up = lax.ppermute(going_up, "sp", [(d, (d + 1) % ways) for d in range(ways)])
+        full = lax.dynamic_update_slice_in_dim(full, going_up, (here - far) % ways * lap, axis=0)
+        if 2 * far < ways:
+            going_down = lax.ppermute(going_down, "sp", [(d, (d - 1) % ways) for d in range(ways)])
+            full = lax.dynamic_update_slice_in_dim(
+                full, going_down, (here + far) % ways * lap, axis=0
+            )
+    all_gates = full
     attention_score_scale = HEAD_DIM ** (-0.5)
     starting = (
         jnp.full((attend_heads, shard_rows), NEGATIVE, jnp.float32),

time: 109 us -> 102 us (0.936)
  blocking collectives: 61.6 us -> 48 us
  starting transfers between devices: 5.05 us -> 9.09 us
  local copies, waits for them, and re-layouts: 5.49 us -> 6.72 us
    all_gather x1 -> x0, blocking collectives: 13.3 us -> none  [shards(): all_gates = lax.all_gather(forget_gate_cumsum[0], 'sp', axis=0, tiled=True)]
    ppermute x0 -> x3, starting transfers between devices: none -> 7.16 us  [the longest x2 5.07 us: shards(): lax.ppermute(going_up, 'sp', [(d, (d + 1) % ways) for d in range(ways)])]
    ppermute x1, starting transfers between devices: 4.97 us -> 1.85 us  [passed_along(): return lax.ppermute(shard, axis, pairs)]
    unnamed x25 -> x23, local copies, waits for them, and re-layouts: 3.25 us -> 4.19 us
  transfers between devices with their start and end apart: 4 -> 7, of which waited for: 1 -> 2; matrix products, arithmetic and copies ran while one was open for 15% -> 17% of each run, Pallas kernels for 0% -> 0%
where the time goes in v1:
time: 102 us; the launch traced here: 101 us
  blocking collectives  48 us (47%)
  between operations  14.1 us (14%)
  waiting for transfers between devices  9.55 us (9%)
  starting transfers between devices  9.09 us (9%)
  matrix products  7.04 us (7%)
  other arithmetic  6.76 us (7%)
  local copies, waits for them, and re-layouts  6.72 us (7%)
    all_gather x1, blocking collectives, entering(): lax.all_gather(a.astype(kind), axis)  14.7 us
    all_gather x1, blocking collectives, shards(): key_rows = lax.all_gather(attention_keys[0], 'sp', axis=0, tiled=True)  12.6 us
    all_gather x1, blocking collectives, shards(): value_rows = lax.all_gather(attention_values[0], 'sp', axis=0, tiled=True)  12.3 us
    unnamed x1, blocking collectives  8.45 us
    reduce_scatter x1, waiting for transfers between devices, shards(): lax.psum_scatter((jnp.dot(state_result, state_columns, preferred_element_...  8.08 us
    ppermute x2, starting transfers between devices, shards(): lax.ppermute(going_up, 'sp', [(d, (d + 1) % ways) for d in range(ways)])  5.07 us
    unnamed x23, local copies, waits for them, and re-layouts  4.19 us
    dot_general x1, matrix products, shards(): jnp.dot(attend_out, attend_columns, preferred_element_type=jnp.float32)  2.87 us
  transfers between devices with their start and end apart: 7, of which 2 were waited for; matrix products, arithmetic and copies ran while one was open for 17% of the time, Pallas kernels for 0%

profile of v1, /device:TPU:0, one launch (start us, length us, event | category | flops | bytes accessed | tf_op | source)
XLA Modules:
  0.0 101.4 jit_solution(11695456559727909698)
XLA Ops:
  6.5 0.7 all-gather.7.cloned.1.call-update
  7.3 3.1 %collective-permute-start.1 = (f32[128,8]{0,1:T(8,128)}, f32[128,8]{0,1:T(8,128)S(1)}, u32[]{:S(2)}, u32[]{:S(2)}) collective-permute-start(f32[128,8]{0,1:T(8,128)} %bitcast.207), channel_id=1, source_target_pairs={{0,8},{8,16},{16,24},{24,0},{1,9},{9,17},{17,25},{25,1},{2,10},{10... | collective-permute-start | bytes 12296 | tf_op jit(solution)/shard_map/ppermute | solution.py:165
  10.4 2.1 %collective-permute-start.2 = (f32[128,8]{0,1:T(8,128)}, f32[128,8]{0,1:T(8,128)S(1)}, u32[]{:S(2)}, u32[]{:S(2)}) collective-permute-start(f32[128,8]{0,1:T(8,128)} %bitcast.208), channel_id=1, source_target_pairs={{0,24},{8,0},{16,8},{24,16},{1,25},{9,1},{17,9},{25,17},{2,26},{10... | collective-permute-start | bytes 12296 | tf_op jit(solution)/shard_map/ppermute | solution.py:168
  12.5 0.7 slice_bitcast_fusion.1
  13.2 0.7 slice_bitcast_fusion
  14.1 1.8 %collective-permute-start = (bf16[3,768]{0,1:T(8,128)(2,1)S(1)}, bf16[3,768]{0,1:T(8,128)(2,1)S(1)}, u32[]{:S(2)}, u32[]{:S(2)}) collective-permute-start(bf16[3,768]{0,1:T(8,128)(2,1)S(1)} %copy.47), channel_id=1, source_target_pairs={{0,8},{8,16},{16,24},{1,9},{9,17},{17,25},{2,10},{10,18},{18,26},{... | collective-permute-start | bytes 13832 | tf_op jit(solution)/shard_map/ppermute | solution.py:16
  16.0 0.7 exponential_negate_fusion
  16.7 0.8 compare_select_fusion
  18.2 0.8 multiply_bitcast_fusion
  18.9 0.9 slice_convert_fusion.3
  19.8 0.8 bitcast_convert_fusion.4
  20.6 0.8 bitcast_convert_fusion.8
  21.4 0.9 copy.54
  22.3 12.6 %all-gather.2 = bf16[1,512,128]{1,2,0:T(8,128)(2,1)S(1)} all-gather(bf16[1,128,128]{1,2,0:T(8,128)(2,1)S(1)} %copy.54), channel_id=4, replica_groups=mesh['sp'=4,'fs'=4,'tp'=2] {'sp'}, dimensions={1}, use_global_device_ids=true | all-gather | bytes 163840 | tf_op jit(solution)/shard_map/all_gather | solution.py:179
  34.9 0.9 copy.55
  35.8 12.3 %all-gather.3 = bf16[1,512,128]{1,2,0:T(8,128)(2,1)S(1)} all-gather(bf16[1,128,128]{1,2,0:T(8,128)(2,1)S(1)} %copy.55), channel_id=5, replica_groups=mesh['sp'=4,'fs'=4,'tp'=2] {'sp'}, dimensions={1}, use_global_device_ids=true | all-gather | bytes 163840 | tf_op jit(solution)/shard_map/all_gather | solution.py:180
  48.0 1.0 %copy.48 = bf16[1,128,512]{1,2,0:T(8,128)(2,1)S(1)} copy(bf16[1,128,512]{2,1,0:T(8,128)(2,1)} %param.22) | data formatting | bytes 262144 | tf_op args[0]
  49.1 0.7 dynamic-slice
  50.7 8.4 %all-reduce = bf16[32]{0:T(256)(128)(2,1)S(1)} all-reduce(bf16[32]{0:T(256)(128)(2,1)S(1)} %dynamic-update-slice), channel_id=2, replica_groups=mesh['sp'=4,'fs'=4,'tp'=2] {'sp'}, use_global_device_ids=true, to_apply=%add | all-reduce | flops 32 | bytes 128
  59.4 2.0 %collective-permute-start.3 = (f32[128,8]{0,1:T(8,128)S(1)}, f32[128,8]{0,1:T(8,128)S(1)}, u32[]{:S(2)}, u32[]{:S(2)}) collective-permute-start(f32[128,8]{0,1:T(8,128)S(1)} %collective-permute-done.1), channel_id=1, source_target_pairs={{0,8},{8,16},{16,24},{24,0},{1,9},{9,17},{17,25},{25,1},{2,10},{10... | collective-permute-start | bytes 12296 | tf_op jit(solution)/shard_map/ppermute | solution.py:165
  61.8 0.6 fusion.23
  62.6 14.7 %all-gather.1 = bf16[32,64,128]{2,1,0:T(8,128)(2,1)S(1)} all-gather(bf16[8,64,128]{2,1,0:T(8,128)(2,1)S(1)} %convolution_convert_fusion), channel_id=3, replica_groups=mesh['sp'=4,'fs'=4,'tp'=2] {'sp'}, dimensions={0}, use_global_device_ids=true | all-gather | bytes 655360 | tf_op jit(solution)/shard_map/all_gather | solution.py:22
  77.7 0.4 copy-done.6
  78.1 0.4 multiply_reduce_fusion
  78.7 2.3 %conditional.1 = ((f32[8,128]{1,0:T(8,128)S(1)}, f32[8,128,64]{1,2,0:T(8,128)S(1)})) conditional(s32[]{:T(128)} %convert_element_type.197, (f32[8,128]{1,0:T(8,128)S(1)}, f32[8,128,64]{1,2,0:T(8,128)S(1)}) %tuple.77, (s32[]{:T(128)}, s32[128]{0:T(128)S(1)}, bf16[512,128]{0,1:T(8,128)(2,1)S(1)}, bf16[1,128,512]{2,1,0:T(8,128)(2,1)S(1)}, ...), branch_computations={%region_4.5_spmd, %region_5.8_spmd.clone.clone} | conditional | flops 140183728 | bytes 8411207 | solution.py:225
  79.3 0.8 fusion.47
  80.1 0.4 fusion.3
  80.5 0.5 fusion.4
  81.1 2.1 %fusion.50 = f32[128,2048]{1,0:T(8,128)S(1)} fusion(bf16[128,512]{0,1:T(8,128)(2,1)S(1)} %fusion.29, bf16[512,2048]{1,0:T(8,128)(2,1)} %all-gather.7.cloned.1.call-done), kind=kOutput, calls=%fused_computation.117 | convolution fusion | flops 268435456 | bytes 3276800 | tf_op jit(solution)/shard_map/dot_general | solution.py:240
  83.2 0.7 all-gather.9.cloned.1.call-done
  83.9 2.9 %fusion.10 = bf16[128,2048]{1,0:T(8,128)(2,1)} fusion(f32[128,2048]{1,0:T(8,128)S(1)} %fusion.50, bf16[128,512]{0,1:T(8,128)(2,1)S(1)} %bitcast.191, bf16[512,2048]{1,0:T(8,128)(2,1)} %all-gather.9.cloned.1.call-done), kind=kOutput, calls=%fused_computation.23 | convolution fusion | flops 268959744 | bytes 3801088 | tf_op jit(solution)/shard_map/dot_general | solution.py:241
  86.8 8.1 %reduce-scatter.2.cloned.1.call-done = bf16[64,2048]{1,0:T(8,128)(2,1)} async-done(((bf16[128,2048]{1,0:T(8,128)(2,1)}), bf16[64,2048]{1,0:T(8,128)(2,1)}) %reduce-scatter.2.cloned.1.call-update) | async-done | bytes 262160 | tf_op jit(solution)/shard_map/reduce_scatter | solution.py:238
  (67 shorter events, 3.3 us)
Async XLA Ops:
  6.5 42.5 %copy-start.7 = (u32[32]{0:T(128)S(1)}, u32[32]{0:T(128)}, u32[]{:S(2)}) copy-start(u32[32]{0:T(128)} %constant.151) | copy-start | bytes 388
  6.5 55.2 %copy-start.2 = (bf16[1,128,128]{2,1,0:T(8,128)(2,1)S(1)}, bf16[1,128,128]{2,1,0:T(8,128)(2,1)}, u32[]{:S(2)}) copy-start(bf16[1,128,128]{2,1,0:T(8,128)(2,1)} %param.23) | copy-start | bytes 98308
  6.5 52.7 %copy-start = (bf16[1,128,512]{2,1,0:T(8,128)(2,1)S(1)}, bf16[1,128,512]{2,1,0:T(8,128)(2,1)}, u32[]{:S(2)}) copy-start(bf16[1,128,512]{2,1,0:T(8,128)(2,1)} %param.25) | copy-start | bytes 393220
  6.5 74.6 %all-gather.7.cloned.1.call-start = ((), (), s32[]{:S(2)}) async-start(), calls=%async_computation.1 | async-start | bytes 2621440 | tf_op jit(solution)/shard_map/all_gather | solution.py:235
  7.3 76.6 %all-gather.9.cloned.1.call-start = ((), (), s32[]{:S(2)}) async-start(), calls=%async_computation.2 | async-start | bytes 2621440 | tf_op jit(solution)/shard_map/all_gather | solution.py:236
  7.3 52.1 %collective-permute-start.1 = (f32[128,8]{0,1:T(8,128)}, f32[128,8]{0,1:T(8,128)S(1)}, u32[]{:S(2)}, u32[]{:S(2)}) collective-permute-start(f32[128,8]{0,1:T(8,128)} %bitcast.207), channel_id=1, source_target_pairs={{0,8},{8,16},{16,24},{24,0},{1,9},{9,17},{17,25},{25,1},{2,10},{10... | collective-permute-start | bytes 12296 | tf_op jit(solution)/shard_map/ppermute | solution.py:165
  10.4 68.2 %collective-permute-start.2 = (f32[128,8]{0,1:T(8,128)}, f32[128,8]{0,1:T(8,128)S(1)}, u32[]{:S(2)}, u32[]{:S(2)}) collective-permute-start(f32[128,8]{0,1:T(8,128)} %bitcast.208), channel_id=1, source_target_pairs={{0,24},{8,0},{16,8},{24,16},{1,25},{9,1},{17,9},{25,17},{2,26},{10... | collective-permute-start | bytes 12296 | tf_op jit(solution)/shard_map/ppermute | solution.py:168
  14.1 47.2 %collective-permute-start = (bf16[3,768]{0,1:T(8,128)(2,1)S(1)}, bf16[3,768]{0,1:T(8,128)(2,1)S(1)}, u32[]{:S(2)}, u32[]{:S(2)}) collective-permute-start(bf16[3,768]{0,1:T(8,128)(2,1)S(1)} %copy.47), channel_id=1, source_target_pairs={{0,8},{8,16},{16,24},{1,9},{9,17},{17,25},{2,10},{10,18},{18,26},{... | collective-permute-start | bytes 13832 | tf_op jit(solution)/shard_map/ppermute | solution.py:16
  16.0 78.9 %reduce-scatter.2.cloned.1.call-start = ((), (), s32[]{:S(2)}) async-start(), calls=%async_computation.3 | async-start | bytes 786432 | tf_op jit(solution)/shard_map/reduce_scatter | solution.py:238
  48.0 14.5 %copy-start.3 = (bf16[1,128,128]{2,1,0:T(8,128)(2,1)S(1)}, bf16[1,128,128]{2,1,0:T(8,128)(2,1)}, u32[]{:S(2)}) copy-start(bf16[1,128,128]{2,1,0:T(8,128)(2,1)} %param.24) | copy-start | bytes 98308
  59.4 19.3 %collective-permute-start.3 = (f32[128,8]{0,1:T(8,128)S(1)}, f32[128,8]{0,1:T(8,128)S(1)}, u32[]{:S(2)}, u32[]{:S(2)}) collective-permute-start(f32[128,8]{0,1:T(8,128)S(1)} %collective-permute-done.1), channel_id=1, source_target_pairs={{0,8},{8,16},{16,24},{24,0},{1,9},{9,17},{17,25},{25,1},{2,10},{10... | collective-permute-start | bytes 12296 | tf_op jit(solution)/shard_map/ppermute | solution.py:165
  77.4 0.7 copy-start.6
  77.5 1.0 %copy-start.5 = (f32[512]{0:T(512)S(1)}, f32[512]{0:T(512)}, u32[]{:S(2)}) copy-start(f32[512]{0:T(512)} %param.33) | copy-start | bytes 6148
  77.5 1.2 %copy-start.1 = (bf16[1,128,512]{2,1,0:T(8,128)(2,1)S(1)}, bf16[1,128,512]{2,1,0:T(8,128)(2,1)}, u32[]{:S(2)}) copy-start(bf16[1,128,512]{2,1,0:T(8,128)(2,1)} %param.34) | copy-start | bytes 393220
  77.5 1.2 %copy-start.4 = (f32[1,128,8]{1,2,0:T(8,128)S(1)}, f32[1,128,8]{1,2,0:T(8,128)}, u32[]{:S(2)}) copy-start(f32[1,128,8]{1,2,0:T(8,128)} %param.37) | copy-start | bytes 12292
Sparse Core Ops, SparseCore 0:
  9.2 37.7 all-gather.6
  48.8 35.0 all-gather.8
  86.9 7.9 reduce-scatter.1
